TPU v7x, 128 devices: a whole 4x4x4 slice. The times are simulated.
128 devices in a mesh: kv: 16 (over z, y), tp: 8 (over x, core).
Axes of the slice: x: 4, y: 4, z: 4, core: 2. Of those that a mesh axis runs over, the one named last changes fastest.
Arguments:
- tokens: bfloat16 [64, 4096], P(None, 'kv'), may hold values from -170 to 170
- mix_gain: float32 [4096], P('kv'), may hold values from 0.1 to 1.9
- w_query: bfloat16 [4096, 2048], P('kv', 'tp'), may hold values from -0.09375 to 0.09375
- w_key: bfloat16 [4096, 512], P('kv', 'tp'), may hold values from -0.09375 to 0.09375
- w_value: bfloat16 [4096, 512], P('kv', 'tp'), may hold values from -0.09375 to 0.09375
- w_forget: bfloat16 [4096, 32], P('kv', 'tp'), may hold values from -0.09375 to 0.09375
- query_gain: float32 [64], replicated, may hold values from 0.1 to 1.9
- key_cache: bfloat16 [64, 8, 64, 16384], P(None, 'tp', None, 'kv'), may hold values from -1300 to 1300
- value_cache: bfloat16 [64, 8, 64, 16384], P(None, 'tp', None, 'kv'), may hold values from -8 to 8
- decay_cache: float32 [64, 32, 16384], P(None, 'tp', 'kv'), may hold values from -2131.92 to 0, as said below
- w_out: bfloat16 [2048, 4096], P('tp', 'kv'), may hold values from -1 to 1
- mlp_gain: float32 [4096], P('kv'), may hold values from 0.1 to 1.9
- w_up: bfloat16 [4096, 16384], P('kv', 'tp'), may hold values from -0.09375 to 0.09375
- w_down: bfloat16 [16384, 4096], P('tp', 'kv'), may hold values from -0.046875 to 0.046875
Outputs:
- layer_out: bfloat16 [64, 4096], P(None, 'kv')
Inputs may be any that keep to these rules, and one draw needn't show every extreme that they name: `decay_cache`: each entry is the sum of the non-positive log forget gates of the later cached positions of its sequence and head: 0 at the last cached position, never smaller at a later position.
All inputs are finite; a program needn't handle non-finite values.
Results may differ from a plain program's by a relative error of at most 0.015.
Values may be sent and summed in bfloat16 or wider, within the bound.
A program may use at most 64 MiB of HBM per device.

v0:
```python
import jax
import jax.numpy as jnp
from jax import lax
from jax.sharding import Mesh
from jax.sharding import PartitionSpec as P

D = 4096
HEAD_DIM = 64
KV = ("kv_0", "kv_1")


EPS = 1e-06


def sent_to_all(array, axis):
    copies = jnp.broadcast_to(array, (lax.axis_size(axis), *array.shape))
    return lax.all_to_all(copies, axis, split_axis=0, concat_axis=0, tiled=True)


def over_copies(array, axis):
    return sent_to_all(array, axis).sum(axis=0)


def in_one(arrays, axis):
    ends = [0]
    for a in arrays:
        ends.append(ends[-1] + a.size)
    subtotal = over_copies(jnp.concatenate([a.ravel() for a in arrays]), axis)
    return tuple((subtotal[b:e].reshape(a.shape) for a, b, e in zip(arrays, ends, ends[1:])))


def gathered_once(array, axis):
    leaves = jax.tree.leaves(array)
    sequence = sorted(range(len(leaves)), key=lambda k: -leaves[k].size)
    width = (1, *leaves[sequence[0]].shape)[-1]
    lines = [
        jnp.pad(leaves[k].reshape(-1), (0, -leaves[k].size % width)).reshape(-1, width)
        for k in sequence
    ]
    both, at, found = (lax.all_gather(jnp.concatenate(lines), axis), 0, {})
    for k, line in zip(sequence, lines):
        piece = both[:, at : at + len(line)].reshape(len(both), -1)
        found[k] = piece[:, : leaves[k].size].reshape(-1, *leaves[k].shape)
        at += len(line)
    numbers = iter(range(len(leaves)))
    return jax.tree.map(lambda _: found[next(numbers)], array)


def merged_by_axis(array, axes, combine):
    for axis in axes:
        pieces = gathered_once(array, axis)
        array = jax.tree.map(lambda part: part[0], pieces)
        for k in range(1, lax.axis_size(axis)):
            array = combine(array, jax.tree.map(lambda part: part[k], pieces))
    return array


def over_copies_2(array, axis):
    return sent_to_all(array, axis).astype(jnp.float32).sum(axis=0)


def cut_along(array, dim, length):
    before, after = (array.shape[:dim], array.shape[dim + 1 :])
    return jnp.moveaxis(array.reshape(*before, length, -1, *after), dim, 0)


def sum_at_owner(array, axis, dim):
    length = lax.axis_size(axis)
    pieces = lax.all_to_all(cut_along(array, dim, length), axis, 0, 0, tiled=True)
    return jnp.sum(pieces, axis=0)


def joined_along(pieces, dim):
    shape = list(pieces.shape[1:])
    shape[dim] *= pieces.shape[0]
    return jnp.moveaxis(pieces, 0, dim).reshape(shape)


def collect(array, axis, dim):
    pieces = sent_to_all(array, axis)
    return joined_along(pieces, dim)


def merge_parts(left_part, right_part):
    peak_score = jnp.maximum(left_part[0], right_part[0])
    left_factor = jnp.exp(left_part[0] - peak_score)
    right_factor = jnp.exp(right_part[0] - peak_score)
    return (
        peak_score,
        left_part[1] * left_factor + right_part[1] * right_factor,
        left_part[2] * left_factor[..., None] + right_part[2] * right_factor[..., None],
    )


def shards(
    tokens,
    mix_gain,
    w_query,
    w_key,
    w_value,
    w_forget,
    query_gain,
    key_cache,
    value_cache,
    decay_cache,
    w_out,
    mlp_gain,
    w_up,
    w_down,
):
    row_count = tokens.shape[0]
    local_heads = w_forget.shape[1]
    local_groups = key_cache.shape[1]
    sharing = local_heads // local_groups
    score_scale = HEAD_DIM ** (-0.5)
    stream = tokens.astype(jnp.float32)
    squares_mix = jnp.sum(stream * stream, axis=1)
    normed_mix = (stream * mix_gain).astype(jnp.bfloat16)
    query_terms = jnp.dot(normed_mix, w_query, preferred_element_type=jnp.float32)
    key_terms = jnp.dot(normed_mix, w_key, preferred_element_type=jnp.float32)
    value_terms = jnp.dot(normed_mix, w_value, preferred_element_type=jnp.float32)
    forget_terms = jnp.dot(normed_mix, w_forget, preferred_element_type=jnp.float32)
    query_raw, key_raw, value_raw, forget_raw, total_mix = in_one(
        (query_terms, key_terms, value_terms, forget_terms, squares_mix), KV
    )
    scale_mix = lax.rsqrt(total_mix / D + EPS)[:, None]
    heads_raw = (scale_mix * query_raw).reshape(row_count, local_heads, HEAD_DIM)
    inverse = lax.rsqrt(jnp.mean(heads_raw * heads_raw, axis=-1, keepdims=True) + EPS)
    query = (heads_raw * inverse * query_gain).astype(jnp.bfloat16)
    query = query.reshape(row_count, local_groups, sharing, HEAD_DIM)
    key_new = (scale_mix * key_raw).reshape(row_count, local_groups, HEAD_DIM).astype(jnp.bfloat16)
    value_new = (
        (scale_mix * value_raw).reshape(row_count, local_groups, HEAD_DIM).astype(jnp.bfloat16)
    )
    log_forget = jax.nn.log_sigmoid(scale_mix * forget_raw).reshape(
        row_count, local_groups, sharing
    )
    decay = decay_cache.reshape(row_count, local_groups, sharing, -1)
    scores = (
        jnp.einsum("bgjd,bgdp->bgjp", query, key_cache, preferred_element_type=jnp.float32)
        * score_scale
    )
    scores = scores + decay + log_forget[..., None]
    own_score = (
        jnp.einsum("bgjd,bgd->bgj", query, key_new, preferred_element_type=jnp.float32)
        * score_scale
    )
    local_peak = jnp.max(scores, axis=-1)
    weights = jnp.exp(scores - local_peak[..., None])
    summed = jnp.einsum(
        "bgjp,bgdp->bgjd",
        weights.astype(jnp.bfloat16),
        value_cache,
        preferred_element_type=jnp.float32,
    )
    far_peak, mass_sum, summed = merged_by_axis(
        (local_peak, jnp.sum(weights, axis=-1), summed), KV, merge_parts
    )
    peak_score = jnp.maximum(far_peak, own_score)
    keep = jnp.exp(far_peak - peak_score)
    mass_sum = mass_sum * keep
    summed = summed * keep[..., None]
    own_weight = jnp.exp(own_score - peak_score)
    totals = mass_sum + own_weight
    own_rounded = lax.optimization_barrier(own_weight.astype(jnp.bfloat16)).astype(jnp.float32)
    summed = summed + own_rounded[..., None] * value_new.astype(jnp.float32)[:, :, None, :]
    head_output = summed / totals[..., None]
    attended = head_output.reshape(row_count, local_heads * HEAD_DIM).astype(jnp.bfloat16)
    attn_terms = jnp.dot(attended, w_out, preferred_element_type=jnp.float32)
    attn_out = over_copies_2(attn_terms.astype(jnp.bfloat16), "tp").astype(jnp.float32)
    attn_rounded = lax.optimization_barrier(attn_out.astype(jnp.bfloat16)).astype(jnp.float32)
    residual = (stream + attn_rounded).astype(jnp.bfloat16)
    residual_wide = residual.astype(jnp.float32)
    squares_mlp = jnp.sum(residual_wide * residual_wide, axis=1)
    normed_mlp = (residual_wide * mlp_gain).astype(jnp.bfloat16)
    up_terms = jnp.dot(normed_mlp, w_up, preferred_element_type=jnp.float32)
    square_columns = jnp.broadcast_to(squares_mlp[:, None], (row_count, lax.axis_size(KV)))
    up_share, total_columns = (sum_at_owner(up_terms, KV, 1), sum_at_owner(square_columns, KV, 1))
    scale_mlp = lax.rsqrt(total_columns[:, 0] / D + EPS)[:, None]
    hidden_share = jnp.square(jax.nn.relu(scale_mlp * up_share)).astype(jnp.bfloat16)
    down_terms = jnp.dot(collect(hidden_share, KV, 1), w_down, preferred_element_type=jnp.float32)
    mlp_out = over_copies_2(down_terms.astype(jnp.bfloat16), "tp").astype(jnp.float32)
    mlp_rounded = lax.optimization_barrier(mlp_out.astype(jnp.bfloat16)).astype(jnp.float32)
    return (residual_wide + mlp_rounded).astype(jnp.bfloat16)


def solution(mesh):
    split = Mesh(mesh.devices.reshape(4, 4, mesh.shape["tp"]), ("kv_0", "kv_1", "tp"))
    return jax.shard_map(
        shards,
        mesh=split,
        in_specs=(
            P(None, KV),
            P(KV),
            P(KV, "tp"),
            P(KV, "tp"),
            P(KV, "tp"),
            P(KV, "tp"),
            P(),
            P(None, "tp", None, KV),
            P(None, "tp", None, KV),
            P(None, "tp", KV),
            P("tp", KV),
            P(KV),
            P(KV, "tp"),
            P("tp", KV),
        ),
        out_specs=P(None, KV),
        check_vma=False,
    )
```

profile of v0, /device:TPU:1, one launch (start us, length us, event | category | flops | bytes accessed | tf_op | source)
XLA Modules:
  0.0 144.4 jit_solution(328288625187221567)
XLA Ops:
  0.0 1.0 fusion.20
  1.0 0.9 fusion.45
  2.0 0.9 fusion.43
  3.0 0.9 fusion.41
  4.0 1.1 convolution_bitcast_fusion.1
  5.2 0.8 broadcast_in_dim.8
  6.0 30.8 %all_to_all.31 = f32[16,1,24896]{2,1,0:T(1,128)S(1)} all-to-all(f32[16,1,24896]{2,1,0:T(1,128)S(1)} %broadcast_in_dim.8), channel_id=1, replica_groups=mesh['kv_0'=4,'kv_1'=4,'tp'=8] {'kv_0','kv_1'}, dimensions={0} | all-to-all | bytes 3186688 | tf_op jit(solution)/shard_map/all_to_all | solution.py:17
  36.8 1.0 reduce_sum.88
  38.2 0.2 multiply_reduce_fusion
  38.4 0.9 multiply_convert_fusion
  39.3 4.9 %fusion.71 = (f32[64,4]{1,0:T(8,128)S(1)}, f32[64,4,1024]{2,1,0:T(4,128)S(1)}) fusion(f32[64,4]{1,0:T(8,128)S(1)} %fusion.37, f32[64,4,1024]{2,1,0:T(4,128)} %param.23, bf16[64,4,64]{2,1,0:T(4,128)(2,1)S(1)} %multiply_convert_fusion, bf16[64,1,64,1024]{3,2,1,0:T(8,128)(2,1)} %param.21), kind=kOutput, calls=%fused_computation.120 | convolution fusion | flops 34602752 | bytes 10520576 | tf_op jit(solution)/shard_map/bgjd,bgdp->bgjp/dot_general | solution.py:140
  44.4 0.5 fusion.13
  44.9 5.7 %fusion = f32[64,4,64]{2,1,0:T(4,128)S(1)} fusion(bf16[64,1,64,1024]{3,2,1,0:T(8,128)(2,1)} %param.22, f32[64,4,1024]{2,1,0:T(4,128)S(1)} %get-tuple-element.49, f32[64,4]{1,0:T(8,128)S(1)} %get-tuple-element.48), kind=kOutput, calls=%fused_computation | convolution fusion | flops 34078720 | bytes 9503744 | tf_op jit(solution)/shard_map/bgjp,bgdp->bgjd/dot_general | solution.py:150
  51.0 10.3 %all-gather.2 = f32[4,264,64]{1,2,0:T(8,128)S(1)} all-gather(f32[1,264,64]{1,2,0:T(8,128)S(1)} %maximum_bitcast_fusion), channel_id=2, replica_groups=mesh['kv_0'=4,'kv_1'=4,'tp'=8] {'kv_0'}, dimensions={0}, use_global_device_ids=true | all-gather | bytes 337920 | tf_op jit(solution)/shard_map/all_gather | solution.py:40
  62.8 10.1 %all-gather.3 = f32[4,264,64]{1,2,0:T(8,128)S(1)} all-gather(f32[1,264,64]{1,2,0:T(8,128)S(1)} %maximum_bitcast_fusion.1), channel_id=3, replica_groups=mesh['kv_0'=4,'kv_1'=4,'tp'=8] {'kv_1'}, dimensions={0}, use_global_device_ids=true | all-gather | bytes 337920 | tf_op jit(solution)/shard_map/all_gather | solution.py:40
  73.3 0.2 fusion.39
  74.1 0.2 squeeze.98
  75.5 0.1 div.29
  75.8 0.1 mul.391
  78.2 0.2 convolution_convert_fusion.1
  78.4 17.5 %all_to_all.32 = bf16[8,64,256]{2,1,0:T(8,128)(2,1)S(1)} all-to-all(bf16[8,64,256]{2,1,0:T(8,128)(2,1)S(1)} %broadcast_in_dim.9), channel_id=1, replica_groups=mesh['kv_0'=4,'kv_1'=4,'tp'=8] {'tp'}, dimensions={0} | all-to-all | bytes 524288 | tf_op jit(solution)/shard_map/all_to_all | solution.py:17
  96.1 0.6 transpose.34
  96.7 3.5 %all-to-all-start.2 = ((f32[16,64,1]{1,2,0:T(1,128)}), f32[16,64,1]{1,2,0:T(1,128)S(1)}, u32[]{:S(2)}, u32[]{:S(2)}) async-start(f32[16,64,1]{1,2,0:T(1,128)} %transpose.34), calls=%async_computation.2 | async-start | bytes 16384 | tf_op jit(solution)/shard_map/all_to_all | solution.py:69
  100.2 0.3 convolution_bitcast_fusion
  100.5 0.8 copy.190
  101.4 5.2 %all-to-all-done.2 = f32[16,64,1]{1,2,0:T(1,128)S(1)} async-done(((f32[16,64,1]{1,2,0:T(1,128)}), f32[16,64,1]{1,2,0:T(1,128)S(1)}, u32[]{:S(2)}, u32[]{:S(2)}) %all-to-all-start.2) | async-done | bytes 4128 | tf_op jit(solution)/shard_map/all_to_all | solution.py:69
  106.5 3.6 %all-to-all-start.3 = ((f32[16,64,128]{2,1,0:T(8,128)}), f32[16,64,128]{2,1,0:T(8,128)S(1)}, u32[]{:S(2)}, u32[]{:S(2)}) async-start(f32[16,64,128]{2,1,0:T(8,128)} %bitcast.165), calls=%async_computation.3 | async-start | bytes 1048576 | tf_op jit(solution)/shard_map/all_to_all | solution.py:69
  110.2 9.2 %all-to-all-done.3 = f32[16,64,128]{2,1,0:T(8,128)S(1)} async-done(((f32[16,64,128]{2,1,0:T(8,128)}), f32[16,64,128]{2,1,0:T(8,128)S(1)}, u32[]{:S(2)}, u32[]{:S(2)}) %all-to-all-start.3) | async-done | bytes 524320 | tf_op jit(solution)/shard_map/all_to_all | solution.py:69
  119.6 10.1 %all_to_all.33 = bf16[16,64,128]{2,1,0:T(8,128)(2,1)S(1)} all-to-all(bf16[16,64,128]{2,1,0:T(8,128)(2,1)S(1)} %broadcast_in_dim.10), channel_id=1, replica_groups=mesh['kv_0'=4,'kv_1'=4,'tp'=8] {'kv_0','kv_1'}, dimensions={0} | all-to-all | bytes 524288 | tf_op jit(solution)/shard_map/all_to_all | solution.py:17
  129.7 0.3 convolution_convert_fusion
  130.1 13.7 %all_to_all.34 = bf16[8,64,256]{2,1,0:T(8,128)(2,1)S(1)} all-to-all(bf16[8,64,256]{2,1,0:T(8,128)(2,1)S(1)} %broadcast_in_dim.11), channel_id=1, replica_groups=mesh['kv_0'=4,'kv_1'=4,'tp'=8] {'tp'}, dimensions={0} | all-to-all | bytes 524288 | tf_op jit(solution)/shard_map/all_to_all | solution.py:17
  143.8 0.6 fusion.24
  (110 shorter events, 7.5 us)
Async XLA Ops:
  0.0 100.2 %copy-start = (bf16[256,2048]{1,0:T(8,128)(2,1)S(1)}, bf16[256,2048]{1,0:T(8,128)(2,1)}, u32[]{:S(2)}) copy-start(bf16[256,2048]{1,0:T(8,128)(2,1)} %param.26) | copy-start | bytes 3145732
  44.9 33.3 %copy-start.3 = (bf16[256,256]{1,0:T(8,128)(2,1)S(1)}, bf16[256,256]{1,0:T(8,128)(2,1)}, u32[]{:S(2)}) copy-start(bf16[256,256]{1,0:T(8,128)(2,1)} %param.24) | copy-start | bytes 393220
  50.6 45.3 %copy-start.1 = (bf16[64,256]{1,0:T(8,128)(2,1)S(1)}, bf16[64,256]{1,0:T(8,128)(2,1)}, u32[]{:S(2)}) copy-start(bf16[64,256]{1,0:T(8,128)(2,1)} %param.14) | copy-start | bytes 98308
  50.6 49.6 %copy-start.4 = (f32[256]{0:T(256)S(1)}, f32[256]{0:T(256)}, u32[]{:S(2)}) copy-start(f32[256]{0:T(256)} %param.25) | copy-start | bytes 3076
  61.4 68.3 %copy-start.2 = (bf16[2048,256]{1,0:T(8,128)(2,1)S(1)}, bf16[2048,256]{1,0:T(8,128)(2,1)}, u32[]{:S(2)}) copy-start(bf16[2048,256]{1,0:T(8,128)(2,1)} %param.27) | copy-start | bytes 3145732
  96.7 9.8 %all-to-all-start.2 = ((f32[16,64,1]{1,2,0:T(1,128)}), f32[16,64,1]{1,2,0:T(1,128)S(1)}, u32[]{:S(2)}, u32[]{:S(2)}) async-start(f32[16,64,1]{1,2,0:T(1,128)} %transpose.34), calls=%async_computation.2 | async-start | bytes 16384 | tf_op jit(solution)/shard_map/all_to_all | solution.py:69
  106.5 12.9 %all-to-all-start.3 = ((f32[16,64,128]{2,1,0:T(8,128)}), f32[16,64,128]{2,1,0:T(8,128)S(1)}, u32[]{:S(2)}, u32[]{:S(2)}) async-start(f32[16,64,128]{2,1,0:T(8,128)} %bitcast.165), calls=%async_computation.3 | async-start | bytes 1048576 | tf_op jit(solution)/shard_map/all_to_all | solution.py:69
where the time goes:
time: 145 us; the launch traced here: 144 us
  blocking collectives  92.5 us (64%)
  matrix products  15.5 us (11%)
  waiting for transfers between devices  14.4 us (10%)
  local copies, waits for them, and re-layouts  9.15 us (6%)
  starting transfers between devices  7.05 us (5%)
  other arithmetic  5.22 us (4%)
    all_to_all x4, blocking collectives, sent_to_all(): return lax.all_to_all(copies, axis, split_axis=0, concat_axis=0, tiled=True)  72.1 us
    all_gather x2, blocking collectives, gathered_once(): both, at, found = (lax.all_gather(jnp.concatenate(lines), axis), 0, {})  20.5 us
    all_to_all x2, waiting for transfers between devices, sum_at_owner(): lax.all_to_all(cut_along(array, dim, length), axis, 0, 0, tiled=True)  14.4 us
    all_to_all x2, starting transfers between devices, sum_at_owner(): lax.all_to_all(cut_along(array, dim, length), axis, 0, 0, tiled=True)  7.05 us
    dot_general x1, matrix products, shards(): jnp.einsum('bgjp,bgdp->bgjd', weights.astype(jnp.bfloat16), value_cache,...  5.74 us
    dot_general x1, matrix products, shards(): jnp.einsum('bgjd,bgdp->bgjp', query, key_cache, preferred_element_type=jn...  4.89 us
  transfers between devices with their start and end apart: 2, of which 2 were waited for; matrix products, arithmetic and copies ran while one was open for 1% of the time, Pallas kernels for 0%

commit v1 on v0

v1 whole, which is shorter than its diff:
```python
import jax
import jax.numpy as jnp
from jax import lax
from jax.experimental import pallas as pl
from jax.experimental.pallas import tpu as pltpu
from jax.sharding import PartitionSpec as P

D = 4096
HEAD_DIM = 64
EPS = 1e-06
F32 = jnp.float32
BF16 = jnp.bfloat16
FAR_FIRST = (2, 1, 3)
SIDE = 4
ROWS = 64
HALF = 32
GROUPS = 16


def near(d):
    return min(d, SIDE - d)


OFFSETS = sorted(
    [(a, b) for a in range(SIDE) for b in range(SIDE) if a or b],
    key=lambda o: -(near(o[0]) + near(o[1])),
)


def dot(a, b):
    return lax.dot_general(a, b, (((1,), (0,)), ((), ())), preferred_element_type=F32)


def dot_t(a, b):
    return lax.dot_general(a, b, (((1,), (1,)), ((), ())), preferred_element_type=F32)


def three(a):
    top = a.astype(BF16)
    rest = a - top.astype(F32)
    mid = rest.astype(BF16)
    low = (rest - mid.astype(F32)).astype(BF16)
    return top, mid, low


def dot_wide(a, b):
    top, mid, low = three(a)
    return (dot(low, b) + dot(mid, b)) + dot(top, b)


def index(shape, dim):
    return lax.broadcasted_iota(jnp.int32, shape, dim)


def ones_where(cond):
    return jnp.where(cond, 1.0, 0.0).astype(BF16)


def kernel(
    tok_h, mixg_h, wq_h, wk_h, wv_h, wf_h, qg_h, k_h, v_h, d_h, wo_h, mlpg_h, wu_h, wd_h,
    out_ref,
    tok, mixg, wq, wk, wv, wf, qg, kb, vb, db, wo, mlpg, wu, wd,
    load_sem,
    t2, spread, pick, same, e_lse, c_lse, t_key, t_value,
    q_send, q_ra, q_mid, q_rb,
    kv_send, kv_ra, kv_mid, kv_rb,
    t_send, t_ra, t_mid, t_rb,
    qx, ox, lx,
    m_send, m_ra, m_mid, m_rb,
    a_pair, a_pr, a_xs, a_xr, a_full,
    n_send, n_ra, n_mid, n_rb,
    up_send, up_recv, hid,
    b_pair, b_pr, b_xs, b_xr, b_full,
    ar_send_sem, ar_recv_sem,
    tile_send_sem, tile_recv_sem,
    tp_send_sem, tp_recv_sem,
    rs_send_sem, rs_recv_sem, ag_send_sem, ag_recv_sem,
):
    kv = lax.axis_index("kv")
    tp = lax.axis_index("tp")
    z, y = kv // SIDE, kv % SIDE
    x, core = tp // 2, tp % 2
    started = []

    def load(k, src, dst):
        copy = pltpu.make_async_copy(src, dst, load_sem.at[k])
        copy.start()
        return copy

    pairs = (
        (tok_h, tok), (mixg_h, mixg), (wq_h, wq), (wk_h, wk), (wv_h, wv), (wf_h, wf), (qg_h, qg),
        (k_h, kb), (d_h, db), (v_h, vb), (wo_h, wo), (mlpg_h, mlpg), (wu_h, wu), (wd_h, wd),
    )
    loads = [load(k, src, dst) for k, (src, dst) in enumerate(pairs)]

    def at_y(d):
        return {"kv": z * SIDE + (y + d) % SIDE}

    def at_z(d):
        return {"kv": ((z + d) % SIDE) * SIDE + y}

    def at_both(dz, dy):
        return {"kv": ((z + dz) % SIDE) * SIDE + (y + dy) % SIDE}

    def at_x(d):
        return {"tp": ((x + d) % SIDE) * 2 + core}

    partner = {"tp": x * 2 + (1 - core)}

    barrier = pltpu.get_barrier_semaphore()
    for dz, dy in OFFSETS:
        pl.semaphore_signal(barrier, inc=1, device_id=at_both(dz, dy))
    for d in FAR_FIRST:
        pl.semaphore_signal(barrier, inc=1, device_id=at_x(d))
    pl.semaphore_signal(barrier, inc=1, device_id=partner)

    def send(src, dst, send_sem, recv_sem, to):
        copy = pltpu.make_async_remote_copy(
            src_ref=src, dst_ref=dst, send_sem=send_sem, recv_sem=recv_sem, device_id=to
        )
        copy.start()
        started.append(copy)
        return copy

    r, l = index((256, 256), 0), index((256, 256), 1)
    t2[...] = ones_where(r % 64 == l % 64)
    same[...] = ones_where(r // 64 == l // 64)
    r, l = index((256, 64), 0), index((256, 64), 1)
    spread[...] = ones_where(r // 4 == l)
    r, l = index((64, 256), 0), index((64, 256), 1)
    pick[...] = ones_where(l // 4 == r)
    r, l = index((128, 256), 0), index((128, 256), 1)
    e_lse[...] = ones_where((r < 12) & (r % 4 == l // 64))
    t_key[...] = ones_where(r == l % 64)
    t_value[...] = ones_where(r - 64 == l % 64)
    r, l = index((256, 128), 0), index((256, 128), 1)
    for part in range(3):
        c_lse[part] = ones_where((r % 64 == 0) & (l == r // 64 + 4 * part))

    for k in range(6):
        loads[k].wait()
    stream = tok[...].astype(F32)
    normed = (stream * mixg[...]).astype(BF16)
    q_send[...] = dot(normed, wq[...]).astype(BF16)
    diagonal = index((ROWS, ROWS), 0) == index((ROWS, ROWS), 1)

    def to_row(column):
        return jnp.sum(jnp.where(diagonal, column, 0.0), axis=0, keepdims=True)

    def to_column(row):
        return jnp.sum(jnp.where(diagonal, row, 0.0), axis=1, keepdims=True)

    t_send[...] = jnp.zeros_like(t_send)
    t_send[0:4, 0:ROWS] = dot_t(wf[...], normed)
    t_send[4:5, 0:ROWS] = to_row(jnp.sum(stream * stream, axis=1, keepdims=True))
    kv_send[:, 0:64] = dot_t(normed, wk[...]).astype(BF16)
    kv_send[:, 64:128] = dot_t(normed, wv[...]).astype(BF16)

    pl.semaphore_wait(barrier, len(OFFSETS) + 3 + 1)

    def first_leg(block, ra, which):
        copies = []
        for d in FAR_FIRST:
            for half, at in ((0, at_y), (1, at_z)):
                sems = (which, 0, half, d - 1)
                copies.append(
                    (half, send(
                        block.at[pl.ds(half * HALF, HALF)], ra.at[half, d - 1],
                        ar_send_sem.at[sems], ar_recv_sem.at[sems], at(d),
                    ))
                )
        return copies

    def second_leg(mid, rb, half, which):
        copies = []
        for d in FAR_FIRST:
            at = (at_z, at_y)[half]
            sems = (which, 1, half, d - 1)
            copies.append(
                send(
                    mid.at[half], rb.at[half, d - 1],
                    ar_send_sem.at[sems], ar_recv_sem.at[sems], at(d),
                )
            )
        return copies

    def wait_half(copies, half):
        for h, copy in copies:
            if h == half:
                copy.wait_recv()

    def four(own, others):
        a, b, c = (others[d].astype(F32) for d in range(3))
        return (own.astype(F32) + b) + (a + c)

    def sum_first(block, ra, mid, rb, copies, which):
        later = []
        for half in range(2):
            wait_half(copies, half)
            own = block[half * HALF : half * HALF + HALF]
            mid[half] = four(own, [ra[half, d] for d in range(3)]).astype(BF16)
            later.append(second_leg(mid, rb, half, which))
        return later

    def sum_second(mid, rb, later):
        halves = []
        for half in range(2):
            for copy in later[half]:
                copy.wait_recv()
            halves.append(four(mid[half], [rb[half, d] for d in range(3)]))
        return jnp.concatenate(halves, axis=0)

    def tile_leg(src, dst, at, which, leg):
        return [
            send(src, dst.at[d - 1], tile_send_sem.at[which, leg, d - 1],
                 tile_recv_sem.at[which, leg, d - 1], at(d))
            for d in FAR_FIRST
        ]

    def tile_sum(own, others, copies):
        for copy in copies:
            copy.wait_recv()
        return four(own[...], [others[d] for d in range(3)])

    q_first = first_leg(q_send, q_ra, 0)
    t_first = tile_leg(t_send, t_ra, at_y, 0, 0)
    kv_first = first_leg(kv_send, kv_ra, 1)

    q_later = sum_first(q_send, q_ra, q_mid, q_rb, q_first, 0)
    t_mid[...] = tile_sum(t_send, t_ra, t_first)
    t_later = tile_leg(t_mid, t_rb, at_z, 0, 1)
    kv_later = sum_first(kv_send, kv_ra, kv_mid, kv_rb, kv_first, 1)

    loads[6].wait()
    gain = dot_wide(qg[...], t_key[0:64, :])

    query_raw = sum_second(q_mid, q_rb, q_later)
    tile = tile_sum(t_mid, t_rb, t_later)
    scale_mix = lax.rsqrt(to_column(tile[4:5, 0:ROWS]) / D + EPS)
    heads_raw = scale_mix * query_raw
    mean_square = dot_wide(heads_raw * heads_raw, same[...]) / HEAD_DIM
    query = (heads_raw * lax.rsqrt(mean_square + EPS) * gain).astype(BF16)
    r, l = index((256, 256), 0), index((256, 256), 1)
    head_mask = l // 64 == r % 4
    row_mask = l // 64 == (r // 4) % 4
    score_scale = HEAD_DIM ** (-0.5)
    rows = dot(spread[...], query) * score_scale
    rows = jnp.where(head_mask, rows, 0.0).astype(BF16)
    qx[...] = jnp.where(row_mask, dot(rows, t2[...]), 0.0).astype(BF16)

    for k in (7, 8, 9):
        loads[k].wait()

    def attend(g, carry):
        at16 = pl.ds(pl.multiple_of(g * 16, 16), 16)
        at256 = pl.ds(pl.multiple_of(g * 256, 256), 256)
        decay = db[pl.ds(pl.multiple_of(g * 4, 4), 4)].reshape(16, 1024)
        scores = dot(qx[at16, :], kb[at256, :]) + decay
        peak = jnp.max(scores, axis=1, keepdims=True)
        weights = jnp.exp(scores - peak)
        mass = jnp.sum(weights, axis=1, keepdims=True)
        summed = dot_t(weights.astype(BF16), vb[at256, :])
        ox[at16, :] = summed / mass
        lx[at16, :] = jnp.broadcast_to(peak + jnp.log(mass), (16, 128))
        return carry

    lax.fori_loop(0, GROUPS, attend, 0, unroll=4)

    kept = jnp.where(row_mask, ox[...], 0.0).astype(BF16)
    folded = jnp.where(head_mask, dot(kept, t2[...]), 0.0).astype(BF16)
    m_send[:, 0:256] = dot(pick[...], folded).astype(BF16)
    top, mid, low = three(lx[...])
    r, l = index((256, 128), 0), index((256, 128), 1)
    parts = jnp.where(l < 4, top.astype(F32), jnp.where(l < 8, mid.astype(F32), low.astype(F32)))
    parts = jnp.where((l < 12) & (l % 4 == r % 4), parts, 0.0).astype(BF16)
    m_send[:, 256:384] = dot(pick[...], parts).astype(BF16)

    m_first = first_leg(m_send, m_ra, 2)

    kv_sum = (scale_mix * sum_second(kv_mid, kv_rb, kv_later)).astype(BF16)
    key_wide = dot(kv_sum, t_key[...])
    value_wide = dot(kv_sum, t_value[...])
    own_score = dot_wide(query.astype(F32) * key_wide, same[...]) * score_scale
    lane_head = index((ROWS, 256), 1) // 64
    forget = jnp.zeros((ROWS, 256), F32)
    for h in range(4):
        forget = jnp.where(lane_head == h, to_column(tile[h : h + 1, 0:ROWS]), forget)
    log_forget = jax.nn.log_sigmoid(scale_mix * forget)

    def merge(blocks):
        lses = [dot(b[:, 256:384], e_lse[...]) for b in blocks]
        peak = jnp.maximum(jnp.maximum(lses[0], lses[2]), jnp.maximum(lses[1], lses[3]))
        factors = [jnp.exp(v - peak) for v in lses]
        terms = [f * b[:, 0:256].astype(F32) for f, b in zip(factors, blocks)]
        mass = (factors[0] + factors[2]) + (factors[1] + factors[3])
        summed = (terms[0] + terms[2]) + (terms[1] + terms[3])
        return peak, mass, summed

    m_later = []
    for half in range(2):
        wait_half(m_first, half)
        peak, mass, summed = merge(
            [m_send[half * HALF : half * HALF + HALF]] + [m_ra[half, d] for d in range(3)]
        )
        m_mid[half, :, 0:256] = (summed / mass).astype(BF16)
        pieces = three(peak + jnp.log(mass))
        packed = dot(pieces[0], c_lse[0]) + dot(pieces[1], c_lse[1]) + dot(pieces[2], c_lse[2])
        m_mid[half, :, 256:384] = packed.astype(BF16)
        m_later.append(second_leg(m_mid, m_rb, half, 2))

    halves = []
    for half in range(2):
        for copy in m_later[half]:
            copy.wait_recv()
        at = slice(half * HALF, half * HALF + HALF)
        peak, mass, summed = merge([m_mid[half]] + [m_rb[half, d] for d in range(3)])
        far = peak + log_forget[at]
        top = jnp.maximum(far, own_score[at])
        keep = jnp.exp(far - top)
        own_weight = jnp.exp(own_score[at] - top)
        own_rounded = own_weight.astype(BF16).astype(F32)
        totals = mass * keep + own_weight
        halves.append((summed * keep + own_rounded * value_wide[at]) / totals)
    attended = jnp.concatenate(halves, axis=0).astype(BF16)

    def over_tp(terms, pair, pr, xs, xr, full, which):
        pair[...] = terms.astype(BF16).reshape(2, HALF, 256)
        copy = send(pair.at[1 - core], pr, tp_send_sem.at[which, 0], tp_recv_sem.at[which, 0], partner)
        copy.wait_recv()
        xs[...] = (pair[core].astype(F32) + pr[...].astype(F32)).astype(BF16)
        copies = [
            send(xs, xr.at[d - 1], tp_send_sem.at[which, d], tp_recv_sem.at[which, d], at_x(d))
            for d in FAR_FIRST
        ]
        for copy in copies:
            copy.wait_recv()
        return four(xs[...], [xr[d] for d in range(3)])

    def both_halves(value, full, which):
        full[core] = value.astype(BF16)
        copy = send(full.at[core], full.at[core], tp_send_sem.at[which, 4], tp_recv_sem.at[which, 4], partner)
        copy.wait_recv()
        return full[...].reshape(ROWS, 256).astype(F32)

    loads[10].wait()
    attn_half = over_tp(dot(attended, wo[...]), a_pair, a_pr, a_xs, a_xr, a_full, 0)
    attn_out = both_halves(attn_half, a_full, 0)
    residual = (stream + attn_out).astype(BF16)
    residual_wide = residual.astype(F32)
    loads[11].wait()
    loads[12].wait()
    normed_mlp = (residual_wide * mlpg[...]).astype(BF16)
    for j in range(8):
        terms = dot(normed_mlp, wu[:, j * 256 : (j + 1) * 256]).astype(BF16)
        up_send[2 * j] = terms[:, 0:128]
        up_send[2 * j + 1] = terms[:, 128:256]
    rs = []
    for k, (dz, dy) in enumerate(OFFSETS):
        to = at_both(dz, dy)
        rs.append(send(up_send.at[to["kv"]], up_recv.at[k], rs_send_sem.at[k], rs_recv_sem.at[k], to))
    n_send[...] = jnp.zeros_like(n_send)
    n_send[0:1, 0:ROWS] = to_row(jnp.sum(residual_wide * residual_wide, axis=1, keepdims=True))
    n_first = tile_leg(n_send, n_ra, at_y, 1, 0)

    up = up_send[kv].astype(F32)
    for k in reversed(range(len(OFFSETS))):
        rs[k].wait_recv()
        up = up + up_recv[k].astype(F32)
    hid[kv] = jnp.square(jnp.maximum(up, 0.0)).astype(BF16)
    ag = []
    for k, (dz, dy) in enumerate(OFFSETS):
        ag.append(send(hid.at[kv], hid.at[kv], ag_send_sem.at[k], ag_recv_sem.at[k], at_both(dz, dy)))
    n_mid[...] = tile_sum(n_send, n_ra, n_first)
    n_later = tile_leg(n_mid, n_rb, at_z, 1, 1)
    loads[13].wait()
    for k in reversed(range(len(OFFSETS))):
        ag[k].wait_recv()
    down = jnp.zeros((ROWS, 256), F32)
    for j in range(8):
        units = jnp.concatenate([hid[2 * j], hid[2 * j + 1]], axis=1)
        down = down + dot(units, wd[j * 256 : (j + 1) * 256, :])
    down_half = over_tp(down, b_pair, b_pr, b_xs, b_xr, b_full, 1)
    squares = tile_sum(n_mid, n_rb, n_later)
    scale_square = 1.0 / (to_column(squares[0:1, 0:ROWS]) / D + EPS)
    half_scale = jnp.where(core == 0, scale_square[0:HALF], scale_square[HALF:ROWS])
    mlp_out = both_halves(down_half * half_scale, b_full, 1)
    out_ref[...] = (residual_wide + mlp_out).astype(BF16)

    for copy in started:
        copy.wait_send()


def shards(
    tokens, mix_gain, w_query, w_key, w_value, w_forget, query_gain,
    key_cache, value_cache, decay_cache, w_out, mlp_gain, w_up, w_down,
):
    operands = (
        tokens, mix_gain.reshape(1, -1), w_query, w_key.T, w_value.T, w_forget.T,
        query_gain.reshape(1, -1), key_cache.reshape(4096, 1024), value_cache.reshape(4096, 1024),
        decay_cache, w_out, mlp_gain.reshape(1, -1), w_up, w_down,
    )
    vmem = pltpu.VMEM
    dma = pltpu.SemaphoreType.DMA

    def two_legs(width):
        return [
            vmem((ROWS, width), BF16), vmem((2, 3, HALF, width), BF16),
            vmem((2, HALF, width), BF16), vmem((2, 3, HALF, width), BF16),
        ]

    def tile_legs():
        return [vmem((8, 128), F32), vmem((3, 8, 128), F32), vmem((8, 128), F32), vmem((3, 8, 128), F32)]

    def tp_bufs():
        return [
            vmem((2, HALF, 256), BF16), vmem((HALF, 256), BF16), vmem((HALF, 256), BF16),
            vmem((3, HALF, 256), BF16), vmem((2, HALF, 256), BF16),
        ]

    scratch = [vmem(a.shape, a.dtype) for a in operands]
    scratch += [dma((len(operands),))]
    scratch += [
        vmem((256, 256), BF16), vmem((256, 64), BF16), vmem((64, 256), BF16), vmem((256, 256), BF16),
        vmem((128, 256), BF16), vmem((3, 256, 128), BF16), vmem((128, 256), BF16), vmem((128, 256), BF16),
    ]
    scratch += two_legs(256) + two_legs(128) + tile_legs()
    scratch += [vmem((256, 256), BF16), vmem((256, 256), F32), vmem((256, 128), F32)]
    scratch += two_legs(384) + tp_bufs() + tile_legs()
    scratch += [vmem((16, ROWS, 128), BF16), vmem((15, ROWS, 128), BF16), vmem((16, ROWS, 128), BF16)]
    scratch += tp_bufs()
    scratch += [dma((3, 2, 2, 3)), dma((3, 2, 2, 3)), dma((2, 2, 3)), dma((2, 2, 3)), dma((2, 5)), dma((2, 5))]
    scratch += [dma((15,))] * 4
    return pl.pallas_call(
        kernel,
        out_shape=jax.ShapeDtypeStruct((ROWS, 256), BF16),
        in_specs=[pl.BlockSpec(memory_space=pl.ANY)] * len(operands),
        out_specs=pl.BlockSpec(memory_space=pltpu.VMEM),
        scratch_shapes=scratch,
        compiler_params=pltpu.CompilerParams(
            collective_id=0, has_side_effects=True, vmem_limit_bytes=60 * 2**20
        ),
    )(*operands)


def solution(mesh):
    return jax.shard_map(
        shards,
        mesh=mesh,
        in_specs=(
            P(None, "kv"),
            P("kv"),
            P("kv", "tp"),
            P("kv", "tp"),
            P("kv", "tp"),
            P("kv", "tp"),
            P(),
            P(None, "tp", None, "kv"),
            P(None, "tp", None, "kv"),
            P(None, "tp", "kv"),
            P("tp", "kv"),
            P("kv"),
            P("kv", "tp"),
            P("tp", "kv"),
        ),
        out_specs=P(None, "kv"),
        check_vma=False,
    )
```

time: 145 us -> 55.7 us (0.38)
  blocking collectives: 92.5 us -> 0 us
  Pallas kernels: 0 us -> 54.1 us
  matrix products: 15.5 us -> 0 us
  waiting for transfers between devices: 14.4 us -> 0 us
  local copies, waits for them, and re-layouts: 9.15 us -> 1.38 us
  starting transfers between devices: 7.05 us -> 0 us
  other arithmetic: 5.22 us -> 0 us
    all_to_all x4 -> x0, blocking collectives: 72.1 us -> none  [sent_to_all(): return lax.all_to_all(copies, axis, split_axis=0, concat_axis=0, tiled=True)]
    pallas_call x0 -> x1, Pallas kernels: none -> 54.1 us  [shards(): pl.pallas_call(kernel, out_shape=jax.ShapeDtypeStruct((ROWS, 256), BF16),...]
    all_gather x2 -> x0, blocking collectives: 20.5 us -> none  [gathered_once(): both, at, found = (lax.all_gather(jnp.concatenate(lines), axis), 0, {})]
    dot_general x10 -> x0, matrix products: 15.5 us -> none  [the longest x1 5.74 us: shards(): jnp.einsum('bgjp,bgdp->bgjd', weights.astype(jnp.bfloat16), value_cache,...]
    all_to_all x2 -> x0, waiting for transfers between devices: 14.4 us -> none  [sum_at_owner(): lax.all_to_all(cut_along(array, dim, length), axis, 0, 0, tiled=True)]
    all_to_all x2 -> x0, starting transfers between devices: 7.05 us -> none  [sum_at_owner(): lax.all_to_all(cut_along(array, dim, length), axis, 0, 0, tiled=True)]
    reduce_sum x9 -> x0, other arithmetic: 2.94 us -> none  [the longest x1 1 us: over_copies(): return sent_to_all(array, axis).sum(axis=0)]
    mul x15 -> x0, local copies, waits for them, and re-layouts: 1.99 us -> none  [the longest x6 0.79 us: merge_parts(): left_part[2] * left_factor[..., None]]
  transfers between devices with their start and end apart: 2 -> 0, of which waited for: 2 -> 0; matrix products, arithmetic and copies ran while one was open for 1% -> 0% of each run, Pallas kernels for 0% -> 0%
where the time goes in v1:
time: 55.7 us; the launch traced here: 55.5 us
  Pallas kernels  54.1 us (97%)
  local copies, waits for them, and re-layouts  1.38 us (2%)
    pallas_call x1, Pallas kernels, shards(): pl.pallas_call(kernel, out_shape=jax.ShapeDtypeStruct((ROWS, 256), BF16),...  54.1 us
    unnamed x1, local copies, waits for them, and re-layouts  1.38 us

profile of v1, /device:TPU:1, one launch (start us, length us, event | category | flops | bytes accessed | tf_op | source)
XLA Modules:
  0.0 55.5 jit_solution(7900039543382060857)
XLA Ops:
  0.0 54.1 %shard_map.136 = bf16[64,256]{1,0:T(8,128)(2,1)} custom-call(bf16[64,256]{1,0:T(8,128)(2,1)} %tok_h.1, f32[1,256]{1,0:T(1,128)} %bitcast.13, bf16[256,256]{1,0:T(8,128)(2,1)} %wq_h.1, bf16[64,256]{1,0:T(8,128)(2,1)} %bitcast.10, bf16[64,256]{1,0:T(8,128)(2,1)} %bitcast.11, bf16[4,256]{1,0:T(4,128)(2,1)} %bitcast.12, f32[1,64]{1,0:T(1,128)} %bitcast.15, ...), custom_call_target="tpu_custom_call" | custom-call | tf_op jit(solution)/shard_map/pallas_call | solution.py:433
  54.2 1.4 %copy.16 = bf16[64,256]{1,0:T(8,128)(2,1)} copy(bf16[64,256]{1,0:T(8,128)(2,1)} %shard_map.136) | data formatting | bytes 65536
